TPU v7x, 32 devices: a whole 2x2x4 slice. The times are simulated.
32 devices in a mesh: sp: 8 (over z, y), dp: 4 (over x, core).
Axes of the slice: x: 2, y: 2, z: 4, core: 2. Of those that a mesh axis runs over, the one named last changes fastest.
Arguments:
- gated: bfloat16 [4, 1024, 3072], P('dp', 'sp'), may hold values from -6 to 6
- values_in: bfloat16 [4, 1024, 3072], P('dp', 'sp'), may hold values from -6 to 6
- upstream: bfloat16 [4, 1024, 3072], P('dp', 'sp'), may hold values from -6 to 6
- gain: float32 [3072], replicated, may hold values from 0.1 to 1.9
- shift: float32 [3072], replicated, may hold values from -3 to 3
- mix_w: bfloat16 [512, 4, 512], P('dp'), may hold values from -0.375 to 0.375
- mix_bias: float32 [4, 512], replicated, may hold values from 0.1 to 1.9
Outputs:
- grad_u: bfloat16 [4, 1024, 3072], P('dp', 'sp')
- grad_v: bfloat16 [4, 1024, 3072], P('dp', 'sp')
- grad_mix: float32 [512, 4, 512], P('dp')
- grad_bias: float32 [4, 512], replicated
- grad_gain: float32 [3072], replicated
- grad_shift: float32 [3072], replicated
All inputs are finite; a program needn't handle non-finite values.
Results may differ from a plain program's by a relative error of at most 0.014.
Values may be sent and summed in bfloat16 or wider, within the bound.
A program may use at most 64 MiB of HBM per device.

v0:
```python
import jax
import jax.numpy as jnp
from jax import lax
from jax.sharding import PartitionSpec as P

SEG = 64


EPS = 1e-05


def span_allowed(span_len):
    places = jnp.arange(span_len)
    return places[:, None] // SEG >= places[None, :] // SEG


def by_groups(normed, mix_grad, mix_w, mix_bias):
    tok_rows, half_width = normed.shape
    dp_count = lax.axis_size("dp")
    sp_count = lax.axis_size("sp")
    span_len, groups = (mix_w.shape[0] * dp_count, mix_w.shape[1])
    group_width = half_width // groups
    channels = half_width // sp_count
    my_group = lax.axis_index("sp") * channels // group_width
    own_rows = lax.dynamic_index_in_dim(mix_w, my_group, 1, keepdims=False)
    gathered = lax.all_gather(own_rows, "dp", axis=0, tiled=True)
    allowed = span_allowed(span_len)
    weights = jnp.where(allowed, gathered, jnp.zeros_like(gathered))
    sent_norm, sent_grad = (
        lax.all_to_all(normed.T, "sp", split_axis=0, concat_axis=1, tiled=True),
        lax.all_to_all(mix_grad.T, "sp", split_axis=0, concat_axis=1, tiled=True),
    )
    seq_len = sent_norm.shape[1]
    blocks = seq_len // span_len
    norm_blocks = sent_norm.reshape(channels, blocks, span_len)
    grad_blocks = sent_grad.reshape(channels, blocks, span_len)
    bias_row = lax.dynamic_index_in_dim(mix_bias, my_group, 0, keepdims=False)
    mixed_f = (
        jnp.einsum("ts,cns->cnt", weights, norm_blocks, preferred_element_type=jnp.float32)
        + bias_row[None, None, :]
    )
    mixed_b = lax.optimization_barrier(mixed_f.astype(jnp.bfloat16))
    back_f = jnp.einsum("ts,cnt->cns", weights, grad_blocks, preferred_element_type=jnp.float32)
    back_b = lax.optimization_barrier(back_f.astype(jnp.bfloat16))
    mixed_tok, back_tok = (
        lax.all_to_all(
            mixed_b.reshape(channels, seq_len), "sp", split_axis=1, concat_axis=0, tiled=True
        ),
        lax.all_to_all(
            back_b.reshape(channels, seq_len), "sp", split_axis=1, concat_axis=0, tiled=True
        ),
    )
    group_term = jnp.einsum(
        "cnt,cns->ts", grad_blocks, norm_blocks, preferred_element_type=jnp.float32
    )
    group_term = group_term * allowed.astype(jnp.float32)
    chosen = (jnp.arange(groups) == my_group).astype(jnp.float32)
    bias_term = chosen[:, None] * jnp.sum(grad_blocks, axis=(0, 1), dtype=jnp.float32)[None, :]
    partial_rows = lax.psum_scatter(
        group_term.astype(jnp.bfloat16), "dp", scatter_dimension=0, tiled=True
    ).astype(jnp.float32)
    placed = chosen[None, :, None] * partial_rows[:, None, :]
    summed = lax.psum_scatter(placed, "sp", scatter_dimension=0, tiled=True)
    grad_mix = lax.all_gather(summed, "sp", axis=0, tiled=True)
    return (mixed_tok.T, back_tok.T, grad_mix, bias_term)


def per_device(gated, values_in, upstream, gain, shift, mix_w, mix_bias):
    raw_values = values_in[0].astype(jnp.float32)
    centred = raw_values - jnp.mean(raw_values, axis=-1, keepdims=True)
    inv_std = lax.rsqrt(jnp.mean(centred * centred, axis=-1, keepdims=True) + EPS)
    unit_v = centred * inv_std
    normed = (unit_v * gain + shift).astype(jnp.bfloat16)
    upstream_f = upstream[0].astype(jnp.float32)
    mix_grad = (upstream_f * gated[0].astype(jnp.float32)).astype(jnp.bfloat16)
    mixed_b, back_b, grad_mix, bias_term = by_groups(normed, mix_grad, mix_w, mix_bias)
    grad_u = (upstream_f * mixed_b.astype(jnp.float32)).astype(jnp.bfloat16)
    grad_normed = back_b.astype(jnp.float32)
    scaled = grad_normed * gain
    grad_v = inv_std * (
        scaled
        - jnp.mean(scaled, axis=-1, keepdims=True)
        - unit_v * jnp.mean(scaled * unit_v, axis=-1, keepdims=True)
    )
    gain_term = jnp.sum(grad_normed * unit_v, axis=0)
    shift_term = jnp.sum(grad_normed, axis=0)
    bias_sum, gain_sum, shift_sum = lax.psum((bias_term, gain_term, shift_term), ("sp", "dp"))
    return (
        grad_u[None],
        grad_v.astype(jnp.bfloat16)[None],
        grad_mix,
        bias_sum,
        gain_sum,
        shift_sum,
    )


def solution(mesh):
    placed = (
        P("dp", "sp", None),
        P("dp", "sp", None),
        P("dp", "sp", None),
        P(),
        P(),
        P("dp", None, None),
        P(),
    )
    return jax.shard_map(
        per_device,
        mesh=mesh,
        in_specs=placed,
        out_specs=(P("dp", "sp", None), P("dp", "sp", None), P("dp", None, None), P(), P(), P()),
        check_vma=False,
    )
```

profile of v0, /device:TPU:0, one launch (start us, length us, event | category | flops | bytes accessed | tf_op | source)
XLA Modules:
  0.0 275.9 jit_solution(8554242832005381242)
XLA Ops:
  7.2 1.6 copy.51
  9.2 1.1 fusion.16
  10.3 7.3 %all-to-all-start.2 = ((bf16[8,384,128]{2,1,0:T(8,128)(2,1)}), bf16[8,384,128]{2,1,0:T(8,128)(2,1)S(1)}, u32[]{:S(2)}, u32[]{:S(2)}) async-start(bf16[8,384,128]{2,1,0:T(8,128)(2,1)} %bitcast.17), calls=%async_computation.2 | async-start | bytes 1572864 | tf_op jit(solution)/shard_map/all_to_all | solution.py:31
  17.9 7.2 %all-gather = bf16[512,1,512]{2,0,1:T(8,128)(2,1)S(1)} all-gather(bf16[128,1,512]{2,0,1:T(8,128)(2,1)S(1)} %copy.69), channel_id=2, replica_groups=mesh['sp'=8,'dp'=4] {'dp'}, dimensions={0}, use_global_device_ids=true | all-gather | bytes 655360 | tf_op jit(solution)/shard_map/all_gather | solution.py:26
  25.1 12.7 %all-to-all-done.2 = bf16[8,384,128]{2,1,0:T(8,128)(2,1)S(1)} async-done(((bf16[8,384,128]{2,1,0:T(8,128)(2,1)}), bf16[8,384,128]{2,1,0:T(8,128)(2,1)S(1)}, u32[]{:S(2)}, u32[]{:S(2)}) %all-to-all-start.2) | async-done | bytes 786464 | tf_op jit(solution)/shard_map/all_to_all | solution.py:31
  38.2 1.6 convolution_convert_fusion
  39.7 2.4 copy.61
  42.1 3.6 %all-to-all-start.3 = ((bf16[384,8,128]{0,2,1:T(8,128)(2,1)}), bf16[384,8,128]{0,2,1:T(8,128)(2,1)S(1)}, u32[]{:S(2)}, u32[]{:S(2)}) async-start(bf16[384,8,128]{0,2,1:T(8,128)(2,1)} %bitcast.20), calls=%async_computation.3 | async-start | bytes 1572864 | tf_op jit(solution)/shard_map/all_to_all | solution.py:49
  46.9 19.1 %all-to-all-done.3 = bf16[384,8,128]{0,2,1:T(8,128)(2,1)S(1)} async-done(((bf16[384,8,128]{0,2,1:T(8,128)(2,1)}), bf16[384,8,128]{0,2,1:T(8,128)(2,1)S(1)}, u32[]{:S(2)}, u32[]{:S(2)}) %all-to-all-start.3) | async-done | bytes 786464 | tf_op jit(solution)/shard_map/all_to_all | solution.py:49
  66.0 0.9 copy-done.3
  66.9 1.3 convert_bitcast_fusion.2
  68.2 1.9 copy.62
  70.1 0.9 fusion.13
  71.0 2.4 fusion.12
  73.4 23.7 %all_to_all.58 = bf16[8,384,128]{2,1,0:T(8,128)(2,1)S(1)} all-to-all(bf16[8,384,128]{2,1,0:T(8,128)(2,1)S(1)} %bitcast.97), channel_id=1, replica_groups=mesh['sp'=8,'dp'=4] {'sp'}, dimensions={0} | all-to-all | bytes 1572864 | tf_op jit(solution)/shard_map/all_to_all | solution.py:30
  97.6 1.4 fusion.18
  99.1 20.8 %reduce-scatter.2.cloned.1.call-done = bf16[128,512]{1,0:T(8,128)(2,1)} async-done(((bf16[512,512]{1,0:T(8,128)(2,1)}), bf16[128,512]{1,0:T(8,128)(2,1)}) %reduce-scatter.2.cloned.1.call-update) | async-done | bytes 131088 | tf_op jit(solution)/shard_map/reduce_scatter | solution.py:59
  119.9 0.9 convert_element_type.104
  120.8 1.2 broadcast_multiply_fusion
  122.0 0.7 constant_dynamic-slice_fusion.1
  122.7 0.7 add_convert_fusion
  123.5 1.2 copy.56
  124.6 5.7 %all-to-all-start.1 = ((bf16[384,8,128]{0,2,1:T(8,128)(2,1)}), bf16[384,8,128]{0,2,1:T(8,128)(2,1)}, u32[]{:S(2)}, u32[]{:S(2)}) async-start(bf16[384,8,128]{0,2,1:T(8,128)(2,1)} %bitcast.98), calls=%async_computation.1 | async-start | bytes 1572864 | tf_op jit(solution)/shard_map/all_to_all | solution.py:46
  131.6 83.9 %all-reduce.4.cloned.1.call-done = f32[128,4,512]{2,1,0:T(4,128)} async-done(((f32[128,4,512]{2,1,0:T(4,128)}), f32[128,4,512]{2,1,0:T(4,128)}) %all-reduce.4.cloned.1.call-update) | async-done | bytes 1048592
  215.5 1.6 constant_dynamic-slice_fusion
  217.4 1.2 copy.65
  218.6 40.8 %all-reduce.1 = (f32[4,512]{1,0:T(4,128)}, f32[3072]{0:T(1024)}, f32[3072]{0:T(1024)}) all-reduce(f32[4,512]{1,0:T(4,128)S(1)} %broadcast_multiply_fusion.1, f32[3072]{0:T(1024)S(1)} %get-tuple-element.24, f32[3072]{0:T(1024)S(1)} %reduce_sum.81), channel_id=1, replica_groups=mesh['sp'=8,'dp'=4] {'sp','dp'}, use_global_device_ids=true, to_apply=%region_8.9 | all-reduce | flops 8192 | bytes 65536 | tf_op jit(solution)/shard_map/psum | solution.py:87
  259.4 2.4 convert_bitcast_fusion.1
  261.8 1.9 copy.57
  263.8 1.0 fusion.15
  264.8 2.3 copy.64
  267.1 2.3 copy.72
  (57 shorter events, 3.8 us)
Async XLA Ops:
  7.2 10.4 %copy-start = (bf16[128,4,512]{2,1,0:T(4,128)(2,1)S(1)}, bf16[128,4,512]{2,1,0:T(4,128)(2,1)}, u32[]{:S(2)}) copy-start(bf16[128,4,512]{2,1,0:T(4,128)(2,1)} %param.12) | copy-start | bytes 1572868
  7.2 1.6 copy-start.8
  8.8 1.5 copy-start.5
  10.3 27.5 %all-to-all-start.2 = ((bf16[8,384,128]{2,1,0:T(8,128)(2,1)}), bf16[8,384,128]{2,1,0:T(8,128)(2,1)S(1)}, u32[]{:S(2)}, u32[]{:S(2)}) async-start(bf16[8,384,128]{2,1,0:T(8,128)(2,1)} %bitcast.17), calls=%async_computation.2 | async-start | bytes 1572864 | tf_op jit(solution)/shard_map/all_to_all | solution.py:31
  37.8 1.9 copy-start.1
  38.1 1.6 copy-start.10
  39.7 6.0 %copy-start.9 = (bf16[1,128,3072]{2,1,0:T(8,128)(2,1)S(1)}, bf16[1,128,3072]{2,1,0:T(8,128)(2,1)}, u32[]{:S(2)}) copy-start(bf16[1,128,3072]{2,1,0:T(8,128)(2,1)} %param.8) | copy-start | bytes 2359300
  42.1 23.9 %all-to-all-start.3 = ((bf16[384,8,128]{0,2,1:T(8,128)(2,1)}), bf16[384,8,128]{0,2,1:T(8,128)(2,1)S(1)}, u32[]{:S(2)}, u32[]{:S(2)}) async-start(bf16[384,8,128]{0,2,1:T(8,128)(2,1)} %bitcast.20), calls=%async_computation.3 | async-start | bytes 1572864 | tf_op jit(solution)/shard_map/all_to_all | solution.py:49
  45.6 74.2 %reduce-scatter.2.cloned.1.call-start = ((), (), s32[]{:S(2)}) async-start(), calls=%async_computation.5 | async-start | bytes 655360 | tf_op jit(solution)/shard_map/reduce_scatter | solution.py:59
  66.0 0.9 copy-start.3
  68.2 1.9 copy-start.12
  70.1 0.9 copy-start.13
  73.4 24.1 %copy-start.11 = (bf16[384,8,128]{0,2,1:T(8,128)(2,1)S(1)}, bf16[384,8,128]{0,2,1:T(8,128)(2,1)}, u32[]{:S(2)}) copy-start(bf16[384,8,128]{0,2,1:T(8,128)(2,1)} %copy-done.10) | copy-start | bytes 2359300
  99.0 116.5 %all-reduce.4.cloned.1.call-start = ((), (), s32[]{:S(2)}) async-start(), calls=%async_computation.7 | async-start | bytes 2097152
  123.5 6.9 %copy-start.14 = (u32[32]{0:T(128)S(1)}, u32[32]{0:T(128)}, u32[]{:S(2)}) copy-start(u32[32]{0:T(128)} %constant.72) | copy-start | bytes 388
  123.5 93.6 %copy-start.2 = (bf16[8,384,128]{2,1,0:T(8,128)(2,1)S(1)}, bf16[8,384,128]{2,1,0:T(8,128)(2,1)}, u32[]{:S(2)}) copy-start(bf16[8,384,128]{2,1,0:T(8,128)(2,1)} %copy-done.1) | copy-start | bytes 2359300
  124.6 92.7 %copy-start.4 = (bf16[384,8,128]{0,2,1:T(8,128)(2,1)S(1)}, bf16[384,8,128]{0,2,1:T(8,128)(2,1)}, u32[]{:S(2)}) copy-start(bf16[384,8,128]{0,2,1:T(8,128)(2,1)} %copy-done.3) | copy-start | bytes 2359300
  124.6 92.8 %copy-start.7 = (bf16[128,3072]{0,1:T(8,128)(2,1)S(1)}, bf16[128,3072]{0,1:T(8,128)(2,1)}, u32[]{:S(2)}) copy-start(bf16[128,3072]{0,1:T(8,128)(2,1)} %get-tuple-element.30) | copy-start | bytes 2359300
  124.6 134.8 %all-to-all-start.1 = ((bf16[384,8,128]{0,2,1:T(8,128)(2,1)}), bf16[384,8,128]{0,2,1:T(8,128)(2,1)}, u32[]{:S(2)}, u32[]{:S(2)}) async-start(bf16[384,8,128]{0,2,1:T(8,128)(2,1)} %bitcast.98), calls=%async_computation.1 | async-start | bytes 1572864 | tf_op jit(solution)/shard_map/all_to_all | solution.py:46
  130.3 136.8 %all-gather.3.cloned.1.call-start = ((), (), s32[]{:S(2)}) async-start(), calls=%async_computation.6 | async-start | bytes 1179648 | tf_op jit(solution)/shard_map/all_gather | solution.py:64
  261.8 2.0 copy-start.6
Sparse Core Ops, SparseCore 0:
  99.1 20.6 reduce-scatter.1
  123.9 91.4 all-reduce.3
  217.6 39.8 all-gather.2
where the time goes:
time: 277 us; the launch traced here: 276 us
  waiting for transfers between devices  136 us (49%)
  blocking collectives  71.7 us (26%)
  local copies, waits for them, and re-layouts  20.2 us (7%)
  starting transfers between devices  16.7 us (6%)
  between operations  14.7 us (5%)
  other arithmetic  12.5 us (5%)
  matrix products  3.68 us (1%)
    unnamed x4, waiting for transfers between devices  83.9 us
    psum x1, blocking collectives, per_device(): lax.psum((bias_term, gain_term, shift_term), ('sp', 'dp'))  40.8 us
    all_to_all x1, blocking collectives, by_groups(): lax.all_to_all(normed.T, 'sp', split_axis=0, concat_axis=1, tiled=True)  23.7 us
    reduce_scatter x1, waiting for transfers between devices, by_groups(): lax.psum_scatter(group_term.astype(jnp.bfloat16), 'dp', scatter_dimension...  20.8 us
    all_to_all x1, waiting for transfers between devices, by_groups(): lax.all_to_all(back_b.reshape(channels, seq_len), 'sp', split_axis=1, con...  19.1 us
    all_to_all x1, waiting for transfers between devices, by_groups(): lax.all_to_all(mix_grad.T, 'sp', split_axis=0, concat_axis=1, tiled=True)  12.7 us
    unnamed x39, local copies, waits for them, and re-layouts  11.2 us
    all_to_all x1, starting transfers between devices, by_groups(): lax.all_to_all(mix_grad.T, 'sp', split_axis=0, concat_axis=1, tiled=True)  7.31 us
  transfers between devices with their start and end apart: 6, of which 4 were waited for; matrix products, arithmetic and copies ran while one was open for 6% of the time, Pallas kernels for 0%

commit v1 on v0

v1 whole, which is shorter than its diff:
```python
import functools

import jax
import jax.numpy as jnp
from jax import lax
from jax.experimental import pallas as pl
from jax.experimental.pallas import tpu as pltpu
from jax.sharding import PartitionSpec as P

SEG = 64


EPS = 1e-05

CHUNK = 16


def kernel(
    dims,
    gated,
    values,
    upstream,
    gain,
    shift,
    mix_w,
    mix_bias,
    grad_u,
    grad_v,
    grad_mix,
    grad_bias,
    grad_gain,
    grad_shift,
    tok_g,
    tok_n,
    recv_g,
    recv_n,
    back_s,
    mixed_s,
    ret_b,
    ret_n,
    w_all,
    term_s,
    term_r,
    dp_sum,
    span_r,
    span_sum,
    group_r,
    acc_gain,
    acc_shift,
    vec_a,
    vec_b,
    vec_c,
    vec_s,
    bias_t,
    sq_send,
    sq_recv,
    dp_send,
    dp_recv,
    sn_send,
    sn_recv,
):
    tok, width, groups, span, dp_count, spans = dims
    half = groups * width
    rows = span // dp_count
    me = lax.axis_index("sp")
    my_span, k = me // groups, me % groups
    d = lax.axis_index("dp")
    f32, bf16 = jnp.float32, jnp.bfloat16

    def sq_id(j):
        return {"sp": my_span * groups + j}

    def dp_id(j):
        return {"dp": j}

    def sn_id(j):
        return {"sp": j * groups + k}

    class Exchange:
        def __init__(self, src, dst, own, count, where, send, recv, slot):
            self.src, self.dst, self.own, self.count = src, dst, own, count
            self.where, self.send, self.recv, self.slot = where, send, recv, slot

        def copy(self, step, to):
            peer = lax.rem(self.own + step, self.count)
            landing = self.own if to else peer
            return pltpu.make_async_remote_copy(
                src_ref=self.src(peer),
                dst_ref=self.dst(landing),
                send_sem=self.send.at[self.slot, step],
                recv_sem=self.recv.at[self.slot, landing],
                device_id=self.where(peer),
                device_id_type=pl.DeviceIdType.MESH,
            )

        def start(self):
            for step in range(1, self.count):
                self.copy(step, True).start()

        def arrive(self):
            for step in range(1, self.count):
                self.copy(step, False).wait_recv()

        def leave(self):
            for step in range(1, self.count):
                self.copy(step, True).wait_send()

    def square(src, dst, slot):
        return Exchange(src, dst, k, groups, sq_id, sq_send, sq_recv, slot)

    def across(src, dst, slot):
        return Exchange(src, dst, d, dp_count, dp_id, dp_send, dp_recv, slot)

    def spanning(src, dst, slot):
        return Exchange(src, dst, my_span, spans, sn_id, sn_send, sn_recv, slot)

    def w_rows(j):
        return w_all.at[pl.ds(pl.multiple_of(j * rows, rows), rows)]

    go_w = across(lambda j: mix_w.at[k], w_rows, 0)
    go_g = square(lambda j: tok_g.at[j], lambda j: recv_g.at[j], 0)
    go_n = square(lambda j: tok_n.at[j], lambda j: recv_n.at[j], 1)
    go_b = square(lambda j: back_s.at[j], lambda j: ret_b.at[j], 2)
    go_m = square(lambda j: mixed_s.at[j], lambda j: ret_n.at[j], 3)
    go_t = across(
        lambda j: term_s.at[pl.ds(pl.multiple_of(j * rows, rows), rows)],
        lambda j: term_r.at[j],
        1,
    )
    go_s = spanning(lambda j: dp_sum, lambda j: span_r.at[j], 0)
    go_q = square(lambda j: span_sum, lambda j: group_r.at[j], 4)
    go_va = across(lambda j: vec_s.at[0], lambda j: vec_a.at[j], 2)
    go_vb = square(lambda j: vec_s.at[1], lambda j: vec_b.at[j], 5)
    go_vc = spanning(lambda j: vec_s.at[2], lambda j: vec_c.at[j], 1)

    barrier = pltpu.get_barrier_semaphore()
    for own, count, where in ((k, groups, sq_id), (d, dp_count, dp_id), (my_span, spans, sn_id)):
        for step in range(1, count):
            pl.semaphore_signal(
                barrier,
                inc=1,
                device_id=where(lax.rem(own + step, count)),
                device_id_type=pl.DeviceIdType.MESH,
            )

    def piece(r):
        return pl.ds(pl.multiple_of(r * CHUNK, CHUNK), CHUNK)

    @pl.loop(0, tok // CHUNK)
    def _(r):
        at = piece(r)
        prod = (upstream[at, :].astype(f32) * gated[at, :].astype(f32)).astype(bf16)
        for g in range(groups):
            tok_g[g, at, :] = prod[:, g * width : (g + 1) * width]

    pl.semaphore_wait(barrier, groups + dp_count + spans - 3)
    go_w.start()
    go_g.start()

    def unit_of(at):
        raw = values[at, :].astype(f32)
        centred = raw - jnp.mean(raw, axis=-1, keepdims=True)
        inv_std = lax.rsqrt(jnp.mean(centred * centred, axis=-1, keepdims=True) + EPS)
        return centred * inv_std, inv_std

    @pl.loop(0, tok // CHUNK)
    def _(r):
        at = piece(r)
        unit, _inv = unit_of(at)
        normed = (unit * gain[...] + shift[...]).astype(bf16)
        for g in range(groups):
            tok_n[g, at, :] = normed[:, g * width : (g + 1) * width]

    go_n.start()
    w_rows(d)[...] = mix_w[k]
    recv_g[k] = tok_g[k]
    recv_n[k] = tok_n[k]
    acc_gain[...] = jnp.zeros_like(acc_gain)
    acc_shift[...] = jnp.zeros_like(acc_shift)
    bias_t[...] = jnp.transpose(jnp.broadcast_to(mix_bias[pl.ds(k, 1), :], (128, span)))

    def allowed(first, count):
        t = first + lax.broadcasted_iota(jnp.int32, (count, span), 0)
        s = lax.broadcasted_iota(jnp.int32, (count, span), 1)
        return lax.div(t, SEG) >= lax.div(s, SEG)

    go_w.arrive()
    for j in range(groups):
        at = slice(j * tok, (j + 1) * tok)
        w_all[at, :] = jnp.where(allowed(j * tok, tok), w_all[at, :].astype(f32), 0.0).astype(bf16)

    go_g.arrive()
    for j in range(groups):
        block = lax.dot_general(
            w_all[:, j * tok : (j + 1) * tok],
            recv_g[...].reshape(span, width),
            (((0,), (0,)), ((), ())),
            preferred_element_type=f32,
        )
        back_s[j] = block.astype(bf16)
    go_b.start()
    ret_b[k] = back_s[k]

    go_n.arrive()
    for j in range(groups):
        block = jnp.dot(
            w_all[j * tok : (j + 1) * tok, :],
            recv_n[...].reshape(span, width),
            preferred_element_type=f32,
        )
        bias = bias_t[j * tok : (j + 1) * tok, :]
        for c in range(width // 128):
            lanes = slice(c * 128, (c + 1) * 128)
            mixed_s[j, :, lanes] = (block[:, lanes] + bias).astype(bf16)
    go_m.start()
    ret_n[k] = mixed_s[k]

    for j in range(groups):
        block = lax.dot_general(
            recv_g[j],
            recv_n[...].reshape(span, width),
            (((1,), (1,)), ((), ())),
            preferred_element_type=f32,
        )
        term_s[j * tok : (j + 1) * tok, :] = jnp.where(allowed(j * tok, tok), block, 0.0).astype(bf16)
    go_t.start()
    term_r[d] = term_s[pl.ds(pl.multiple_of(d * rows, rows), rows), :]
    bias_sum = lax.dot_general(
        jnp.ones((8, width), bf16),
        recv_g[...].reshape(span, width),
        (((1,), (1,)), ((), ())),
        preferred_element_type=f32,
    )[0:1]

    go_b.arrive()

    @pl.loop(0, tok // CHUNK)
    def _(r):
        at = piece(r)
        unit, inv_std = unit_of(at)
        grad_normed = jnp.concatenate([ret_b[g, at, :] for g in range(groups)], axis=1).astype(f32)
        acc_gain[...] += grad_normed * unit
        acc_shift[...] += grad_normed
        scaled = grad_normed * gain[...]
        grad_v[at, :] = (
            inv_std
            * (
                scaled
                - jnp.mean(scaled, axis=-1, keepdims=True)
                - unit * jnp.mean(scaled * unit, axis=-1, keepdims=True)
            )
        ).astype(bf16)

    parts = half // span
    gain_sum = jnp.sum(acc_gain[...], axis=0, keepdims=True)
    shift_sum = jnp.sum(acc_shift[...], axis=0, keepdims=True)
    for i in range(parts):
        vec_s[0, i : i + 1, :] = gain_sum[:, i * span : (i + 1) * span]
        vec_s[0, parts + i : parts + i + 1, :] = shift_sum[:, i * span : (i + 1) * span]
    for g in range(groups):
        vec_s[0, 2 * parts + g : 2 * parts + g + 1, :] = jnp.where(k == g, bias_sum, 0.0)
    go_va.start()
    vec_a[d] = vec_s[0]

    def total(ref, count):
        out = ref[0].astype(f32)
        for i in range(1, count):
            out = out + ref[i].astype(f32)
        return out

    go_t.arrive()
    dp_sum[...] = total(term_r, dp_count).astype(bf16)
    go_s.start()
    span_r[my_span] = dp_sum[...]

    go_va.arrive()
    vec_s[1] = total(vec_a, dp_count)
    go_vb.start()
    vec_b[k] = vec_s[1]

    go_s.arrive()
    span_sum[...] = total(span_r, spans).astype(bf16)
    go_q.start()
    group_r[k] = span_sum[...]

    go_vb.arrive()
    vec_s[2] = total(vec_b, groups)
    go_vc.start()
    vec_c[my_span] = vec_s[2]

    go_m.arrive()

    @pl.loop(0, tok // CHUNK)
    def _(r):
        at = piece(r)
        mixed = jnp.concatenate([ret_n[g, at, :] for g in range(groups)], axis=1).astype(f32)
        grad_u[at, :] = (upstream[at, :].astype(f32) * mixed).astype(bf16)

    go_vc.arrive()
    summed = total(vec_c, spans)
    for i in range(parts):
        grad_gain[:, i * span : (i + 1) * span] = summed[i : i + 1, :]
        grad_shift[:, i * span : (i + 1) * span] = summed[parts + i : parts + i + 1, :]
    grad_bias[...] = summed[2 * parts : 2 * parts + groups, :]

    go_q.arrive()
    for g in range(groups):
        grad_mix[g] = group_r[g].astype(f32)

    for go in (go_w, go_g, go_n, go_b, go_m, go_t, go_s, go_q, go_va, go_vb, go_vc):
        go.leave()


def per_device(gated, values_in, upstream, gain, shift, mix_w, mix_bias):
    dp_count = lax.axis_size("dp")
    sp_count = lax.axis_size("sp")
    tok, half = gated.shape[1:]
    rows, groups, span = mix_w.shape
    width = half // groups
    assert span == groups * tok
    spans = sp_count // groups
    vec_rows = 2 * (half // span) + groups
    f32, bf16 = jnp.float32, jnp.bfloat16
    block = pltpu.VMEM((groups, tok, width), bf16)
    scratch = (
        [block] * 8
        + [
            pltpu.VMEM((span, span), bf16),
            pltpu.VMEM((span, span), bf16),
            pltpu.VMEM((dp_count, rows, span), bf16),
            pltpu.VMEM((rows, span), bf16),
            pltpu.VMEM((spans, rows, span), bf16),
            pltpu.VMEM((rows, span), bf16),
            pltpu.VMEM((groups, rows, span), bf16),
            pltpu.VMEM((CHUNK, half), f32),
            pltpu.VMEM((CHUNK, half), f32),
            pltpu.VMEM((dp_count, vec_rows, span), f32),
            pltpu.VMEM((groups, vec_rows, span), f32),
            pltpu.VMEM((spans, vec_rows, span), f32),
            pltpu.VMEM((3, vec_rows, span), f32),
            pltpu.VMEM((span, 128), f32),
        ]
        + [pltpu.SemaphoreType.DMA((6, groups))] * 2
        + [pltpu.SemaphoreType.DMA((3, dp_count))] * 2
        + [pltpu.SemaphoreType.DMA((2, spans))] * 2
    )
    vmem = pl.BlockSpec(memory_space=pltpu.VMEM)
    out = pl.pallas_call(
        functools.partial(kernel, (tok, width, groups, span, dp_count, spans)),
        out_shape=(
            jax.ShapeDtypeStruct((tok, half), bf16),
            jax.ShapeDtypeStruct((tok, half), bf16),
            jax.ShapeDtypeStruct((groups, rows, span), f32),
            jax.ShapeDtypeStruct((groups, span), f32),
            jax.ShapeDtypeStruct((1, half), f32),
            jax.ShapeDtypeStruct((1, half), f32),
        ),
        in_specs=[vmem] * 7,
        out_specs=[vmem] * 6,
        scratch_shapes=scratch,
        compiler_params=pltpu.CompilerParams(
            collective_id=0, has_side_effects=True, vmem_limit_bytes=48 * 1024 * 1024
        ),
    )(
        gated[0],
        values_in[0],
        upstream[0],
        gain[None],
        shift[None],
        jnp.transpose(mix_w, (1, 0, 2)),
        mix_bias,
    )
    return (
        out[0][None],
        out[1][None],
        jnp.transpose(out[2], (1, 0, 2)),
        out[3],
        out[4][0],
        out[5][0],
    )


def solution(mesh):
    placed = (
        P("dp", "sp", None),
        P("dp", "sp", None),
        P("dp", "sp", None),
        P(),
        P(),
        P("dp", None, None),
        P(),
    )
    return jax.shard_map(
        per_device,
        mesh=mesh,
        in_specs=placed,
        out_specs=(P("dp", "sp", None), P("dp", "sp", None), P("dp", None, None), P(), P(), P()),
        check_vma=False,
    )
```

time: 277 us -> 61.5 us (0.22)
  waiting for transfers between devices: 136 us -> 0 us
  blocking collectives: 71.7 us -> 0 us
  Pallas kernels: 0 us -> 51.9 us
  starting transfers between devices: 16.7 us -> 0 us
  between operations: 14.7 us -> 0.69 us
  other arithmetic: 12.5 us -> 0 us
  local copies, waits for them, and re-layouts: 20.2 us -> 8.73 us
  matrix products: 3.68 us -> 0 us
    unnamed x4 -> x0, waiting for transfers between devices: 83.9 us -> none
    pallas_call x0 -> x1, Pallas kernels: none -> 51.9 us  [per_device(): pl.pallas_call(functools.partial(kernel, (tok, width, groups, span, dp_co...]
    psum x1 -> x0, blocking collectives: 40.8 us -> none  [per_device(): lax.psum((bias_term, gain_term, shift_term), ('sp', 'dp'))]
    all_to_all x3 -> x0, waiting for transfers between devices: 31.8 us -> none  [the longest x1 19.1 us: by_groups(): lax.all_to_all(back_b.reshape(channels, seq_len), 'sp', split_axis=1, con...]
    all_to_all x1 -> x0, blocking collectives: 23.7 us -> none  [by_groups(): lax.all_to_all(normed.T, 'sp', split_axis=0, concat_axis=1, tiled=True)]
    reduce_scatter x1 -> x0, waiting for transfers between devices: 20.8 us -> none  [by_groups(): lax.psum_scatter(group_term.astype(jnp.bfloat16), 'dp', scatter_dimension...]
    all_to_all x3 -> x0, starting transfers between devices: 16.5 us -> none  [the longest x1 7.31 us: by_groups(): lax.all_to_all(mix_grad.T, 'sp', split_axis=0, concat_axis=1, tiled=True)]
    convert_element_type x7 -> x0, other arithmetic: 9.16 us -> none  [the longest x2 3.47 us: per_device(): grad_u = (upstream_f * mixed_b.astype(jnp.float32)).astype(jnp.bfloat16)]
  transfers between devices with their start and end apart: 6 -> 0, of which waited for: 4 -> 0; matrix products, arithmetic and copies ran while one was open for 6% -> 0% of each run, Pallas kernels for 0% -> 0%
where the time goes in v1:
time: 61.5 us; the launch traced here: 61.3 us
  Pallas kernels  51.9 us (84%)
  local copies, waits for them, and re-layouts  8.73 us (14%)
  between operations  0.69 us (1%)
    pallas_call x1, Pallas kernels, per_device(): pl.pallas_call(functools.partial(kernel, (tok, width, groups, span, dp_co...  51.9 us
    unnamed x19, local copies, waits for them, and re-layouts  8.73 us

profile of v1, /device:TPU:0, one launch (start us, length us, event | category | flops | bytes accessed | tf_op | source)
XLA Modules:
  0.0 61.3 jit_solution(18298358416637889701)
XLA Ops:
  0.6 0.0 copy-start
  0.6 0.0 copy-start.3
  0.7 0.0 copy-start.4
  0.7 0.0 copy-start.5
  0.7 1.2 %copy.16 = bf16[128,4,512]{2,0,1:T(8,128)(2,1)S(1)} copy(bf16[128,4,512]{2,1,0:T(4,128)(2,1)} %param.12) | data formatting | bytes 1048576 | tf_op args[5]
  1.9 0.0 copy-done
  1.9 0.0 copy-done.3
  1.9 0.0 copy-done.4
  1.9 0.0 copy-done.5
  1.9 0.0 copy-start.1
  1.9 1.1 %copy-done.1 = bf16[1,128,3072]{2,1,0:T(8,128)(2,1)S(1)} copy-done((bf16[1,128,3072]{2,1,0:T(8,128)(2,1)S(1)}, bf16[1,128,3072]{2,1,0:T(8,128)(2,1)}, u32[]{:S(2)}) %copy-start.1) | copy-done | bytes 786456
  3.1 0.0 copy-start.2
  3.1 1.1 %copy-done.2 = bf16[1,128,3072]{2,1,0:T(8,128)(2,1)S(1)} copy-done((bf16[1,128,3072]{2,1,0:T(8,128)(2,1)S(1)}, bf16[1,128,3072]{2,1,0:T(8,128)(2,1)}, u32[]{:S(2)}) %copy-start.2) | copy-done | bytes 786456
  4.2 51.9 %shard_map.118 = (bf16[128,3072]{1,0:T(8,128)(2,1)S(1)}, bf16[128,3072]{1,0:T(8,128)(2,1)S(1)}, f32[4,128,512]{2,1,0:T(8,128)S(1)}, f32[4,512]{1,0:T(4,128)S(1)}...) custom-call(bf16[128,3072]{1,0:T(8,128)(2,1)S(1)} %bitcast.17, bf16[128,3072]{1,0:T(8,128)(2,1)S(1)} %bitcast.18, ...), custom_call_target="tpu_custom_call" | custom-call | tf_op jit(solution)/shard_map/pallas_call | solution.py:348
  56.1 1.6 %copy.14 = f32[128,4,512]{2,1,0:T(4,128)} copy(f32[128,4,512]{2,0,1:T(8,128)S(1)} %bitcast.14) | data formatting | bytes 2097152
  57.7 0.9 %copy.22 = bf16[1,128,3072]{2,1,0:T(8,128)(2,1)} copy(bf16[1,128,3072]{2,1,0:T(8,128)(2,1)S(1)} %bitcast.16) | data formatting | bytes 1572864
  58.6 0.9 %copy.23 = bf16[1,128,3072]{2,1,0:T(8,128)(2,1)} copy(bf16[1,128,3072]{2,1,0:T(8,128)(2,1)S(1)} %bitcast.15) | data formatting | bytes 1572864
  59.5 0.6 copy.24
  60.1 0.6 copy.25
  60.7 0.6 copy.26
Async XLA Ops:
  0.6 1.3 %copy-start = (bf16[1,128,3072]{2,1,0:T(8,128)(2,1)S(1)}, bf16[1,128,3072]{2,1,0:T(8,128)(2,1)}, u32[]{:S(2)}) copy-start(bf16[1,128,3072]{2,1,0:T(8,128)(2,1)} %param.7) | copy-start | bytes 2359300
  0.6 1.3 %copy-start.3 = (f32[3072]{0:T(1024)S(1)}, f32[3072]{0:T(1024)}, u32[]{:S(2)}) copy-start(f32[3072]{0:T(1024)} %param.10) | copy-start | bytes 36868
  0.7 1.3 %copy-start.4 = (f32[3072]{0:T(1024)S(1)}, f32[3072]{0:T(1024)}, u32[]{:S(2)}) copy-start(f32[3072]{0:T(1024)} %param.11) | copy-start | bytes 36868
  0.7 1.3 %copy-start.5 = (f32[4,512]{1,0:T(4,128)S(1)}, f32[4,512]{1,0:T(4,128)}, u32[]{:S(2)}) copy-start(f32[4,512]{1,0:T(4,128)} %mix_bias.1) | copy-start | bytes 24580
  1.9 1.1 %copy-start.1 = (bf16[1,128,3072]{2,1,0:T(8,128)(2,1)S(1)}, bf16[1,128,3072]{2,1,0:T(8,128)(2,1)}, u32[]{:S(2)}) copy-start(bf16[1,128,3072]{2,1,0:T(8,128)(2,1)} %param.8) | copy-start | bytes 2359300
  3.1 1.1 %copy-start.2 = (bf16[1,128,3072]{2,1,0:T(8,128)(2,1)S(1)}, bf16[1,128,3072]{2,1,0:T(8,128)(2,1)}, u32[]{:S(2)}) copy-start(bf16[1,128,3072]{2,1,0:T(8,128)(2,1)} %param.9) | copy-start | bytes 2359300

commit v2 on v1

--- a/solution.py
+++ b/solution.py
@@ -17,19 +17,21 @@
 
 def kernel(
     dims,
-    gated,
-    values,
-    upstream,
+    gated_in,
+    values_hbm,
+    upstream_in,
     gain,
     shift,
     mix_w,
     mix_bias,
     grad_u,
     grad_v,
-    grad_mix,
-    grad_bias,
-    grad_gain,
-    grad_shift,
+    group_r,
+    summed,
+    gated,
+    values,
+    upstream,
+    my_w,
     tok_g,
     tok_n,
     recv_g,
@@ -44,7 +46,6 @@
     dp_sum,
     span_r,
     span_sum,
-    group_r,
     acc_gain,
     acc_shift,
     vec_a,
@@ -58,6 +59,7 @@
     dp_recv,
     sn_send,
     sn_recv,
+    in_sem,
 ):
     tok, width, groups, span, dp_count, spans = dims
     half = groups * width
@@ -117,7 +119,7 @@
     def w_rows(j):
         return w_all.at[pl.ds(pl.multiple_of(j * rows, rows), rows)]
 
-    go_w = across(lambda j: mix_w.at[k], w_rows, 0)
+    go_w = across(lambda j: my_w, w_rows, 0)
     go_g = square(lambda j: tok_g.at[j], lambda j: recv_g.at[j], 0)
     go_n = square(lambda j: tok_n.at[j], lambda j: recv_n.at[j], 1)
     go_b = square(lambda j: back_s.at[j], lambda j: ret_b.at[j], 2)
@@ -133,6 +135,15 @@
     go_vb = square(lambda j: vec_s.at[1], lambda j: vec_b.at[j], 5)
     go_vc = spanning(lambda j: vec_s.at[2], lambda j: vec_c.at[j], 1)
 
+    fetches = [
+        pltpu.make_async_copy(src, dst, in_sem.at[i])
+        for i, (src, dst) in enumerate(
+            ((gated_in, gated), (upstream_in, upstream), (values_hbm, values))
+        )
+    ]
+    for fetch in fetches:
+        fetch.start()
+
     barrier = pltpu.get_barrier_semaphore()
     for own, count, where in ((k, groups, sq_id), (d, dp_count, dp_id), (my_span, spans, sn_id)):
         for step in range(1, count):
@@ -146,6 +157,9 @@
     def piece(r):
         return pl.ds(pl.multiple_of(r * CHUNK, CHUNK), CHUNK)
 
+    fetches[0].wait()
+    fetches[1].wait()
+
     @pl.loop(0, tok // CHUNK)
     def _(r):
         at = piece(r)
@@ -154,8 +168,19 @@
             tok_g[g, at, :] = prod[:, g * width : (g + 1) * width]
 
     pl.semaphore_wait(barrier, groups + dp_count + spans - 3)
+    go_g.start()
+
+    @pl.loop(0, rows // CHUNK)
+    def _(r):
+        at = piece(r)
+        whole = mix_w[at].astype(f32)
+        rows_of = whole[:, 0, :]
+        for g in range(1, groups):
+            rows_of = jnp.where(k == g, whole[:, g, :], rows_of)
+        my_w[at, :] = rows_of.astype(bf16)
+
     go_w.start()
-    go_g.start()
+    fetches[2].wait()
 
     def unit_of(at):
         raw = values[at, :].astype(f32)
@@ -172,7 +197,7 @@
             tok_n[g, at, :] = normed[:, g * width : (g + 1) * width]
 
     go_n.start()
-    w_rows(d)[...] = mix_w[k]
+    w_rows(d)[...] = my_w[...]
     recv_g[k] = tok_g[k]
     recv_n[k] = tok_n[k]
     acc_gain[...] = jnp.zeros_like(acc_gain)
@@ -202,6 +227,16 @@
     ret_b[k] = back_s[k]
 
     go_n.arrive()
+    for j in range(groups):
+        block = lax.dot_general(
+            recv_g[j],
+            recv_n[...].reshape(span, width),
+            (((1,), (1,)), ((), ())),
+            preferred_element_type=f32,
+        )
+        term_s[j * tok : (j + 1) * tok, :] = jnp.where(allowed(j * tok, tok), block, 0.0).astype(bf16)
+    go_t.start()
+    term_r[d] = term_s[pl.ds(pl.multiple_of(d * rows, rows), rows), :]
     for j in range(groups):
         block = jnp.dot(
             w_all[j * tok : (j + 1) * tok, :],
@@ -215,16 +250,6 @@
     go_m.start()
     ret_n[k] = mixed_s[k]
 
-    for j in range(groups):
-        block = lax.dot_general(
-            recv_g[j],
-            recv_n[...].reshape(span, width),
-            (((1,), (1,)), ((), ())),
-            preferred_element_type=f32,
-        )
-        term_s[j * tok : (j + 1) * tok, :] = jnp.where(allowed(j * tok, tok), block, 0.0).astype(bf16)
-    go_t.start()
-    term_r[d] = term_s[pl.ds(pl.multiple_of(d * rows, rows), rows), :]
     bias_sum = lax.dot_general(
         jnp.ones((8, width), bf16),
         recv_g[...].reshape(span, width),
@@ -297,18 +322,32 @@
         grad_u[at, :] = (upstream[at, :].astype(f32) * mixed).astype(bf16)
 
     go_vc.arrive()
-    summed = total(vec_c, spans)
+    summed[...] = total(vec_c, spans)
+    go_q.arrive()
+
+    for go in (go_w, go_g, go_n, go_b, go_m, go_t, go_s, go_q, go_va, go_vb, go_vc):
+        go.leave()
+
+
+def finish(
+    u_in, v_in, group_r, summed, grad_u, grad_v, grad_mix, grad_bias, grad_gain, grad_shift, sems
+):
+    copies = [
+        pltpu.make_async_copy(u_in, grad_u, sems.at[0]),
+        pltpu.make_async_copy(v_in, grad_v, sems.at[1]),
+    ]
+    for copy in copies:
+        copy.start()
+    groups, span = grad_bias.shape
+    parts = grad_gain.shape[-1] // span
+    for g in range(groups):
+        grad_mix[:, g, :] = group_r[g].astype(jnp.float32)
     for i in range(parts):
         grad_gain[:, i * span : (i + 1) * span] = summed[i : i + 1, :]
         grad_shift[:, i * span : (i + 1) * span] = summed[parts + i : parts + i + 1, :]
     grad_bias[...] = summed[2 * parts : 2 * parts + groups, :]
-
-    go_q.arrive()
-    for g in range(groups):
-        grad_mix[g] = group_r[g].astype(f32)
-
-    for go in (go_w, go_g, go_n, go_b, go_m, go_t, go_s, go_q, go_va, go_vb, go_vc):
-        go.leave()
+    for copy in copies:
+        copy.wait()
 
 
 def per_device(gated, values_in, upstream, gain, shift, mix_w, mix_bias):
@@ -322,8 +361,11 @@
     vec_rows = 2 * (half // span) + groups
     f32, bf16 = jnp.float32, jnp.bfloat16
     block = pltpu.VMEM((groups, tok, width), bf16)
+    hbm = pl.BlockSpec(memory_space=pltpu.HBM)
     scratch = (
-        [block] * 8
+        [pltpu.VMEM((tok, half), bf16)] * 3
+        + [pltpu.VMEM((rows, span), bf16)]
+        + [block] * 8
         + [
             pltpu.VMEM((span, span), bf16),
             pltpu.VMEM((span, span), bf16),
@@ -331,7 +373,6 @@
             pltpu.VMEM((rows, span), bf16),
             pltpu.VMEM((spans, rows, span), bf16),
             pltpu.VMEM((rows, span), bf16),
-            pltpu.VMEM((groups, rows, span), bf16),
             pltpu.VMEM((CHUNK, half), f32),
             pltpu.VMEM((CHUNK, half), f32),
             pltpu.VMEM((dp_count, vec_rows, span), f32),
@@ -343,6 +384,7 @@
         + [pltpu.SemaphoreType.DMA((6, groups))] * 2
         + [pltpu.SemaphoreType.DMA((3, dp_count))] * 2
         + [pltpu.SemaphoreType.DMA((2, spans))] * 2
+        + [pltpu.SemaphoreType.DMA((3,))]
     )
     vmem = pl.BlockSpec(memory_space=pltpu.VMEM)
     out = pl.pallas_call(
@@ -350,16 +392,14 @@
         out_shape=(
             jax.ShapeDtypeStruct((tok, half), bf16),
             jax.ShapeDtypeStruct((tok, half), bf16),
-            jax.ShapeDtypeStruct((groups, rows, span), f32),
-            jax.ShapeDtypeStruct((groups, span), f32),
-            jax.ShapeDtypeStruct((1, half), f32),
-            jax.ShapeDtypeStruct((1, half), f32),
+            jax.ShapeDtypeStruct((groups, rows, span), bf16),
+            jax.ShapeDtypeStruct((vec_rows, span), f32),
         ),
-        in_specs=[vmem] * 7,
-        out_specs=[vmem] * 6,
+        in_specs=[hbm] * 3 + [vmem] * 4,
+        out_specs=[vmem] * 4,
         scratch_shapes=scratch,
         compiler_params=pltpu.CompilerParams(
-            collective_id=0, has_side_effects=True, vmem_limit_bytes=48 * 1024 * 1024
+            collective_id=0, has_side_effects=True, vmem_limit_bytes=60 * 1024 * 1024
         ),
     )(
         gated[0],
@@ -367,17 +407,25 @@
         upstream[0],
         gain[None],
         shift[None],
-        jnp.transpose(mix_w, (1, 0, 2)),
+        mix_w,
         mix_bias,
     )
-    return (
-        out[0][None],
-        out[1][None],
-        jnp.transpose(out[2], (1, 0, 2)),
-        out[3],
-        out[4][0],
-        out[5][0],
-    )
+    u, v, mix, bias, gain_g, shift_g = pl.pallas_call(
+        finish,
+        out_shape=(
+            jax.ShapeDtypeStruct((tok, half), bf16),
+            jax.ShapeDtypeStruct((tok, half), bf16),
+            jax.ShapeDtypeStruct((rows, groups, span), f32),
+            jax.ShapeDtypeStruct((groups, span), f32),
+            jax.ShapeDtypeStruct((1, half), f32),
+            jax.ShapeDtypeStruct((1, half), f32),
+        ),
+        in_specs=[vmem] * 4,
+        out_specs=[hbm] * 2 + [vmem] * 4,
+        scratch_shapes=[pltpu.SemaphoreType.DMA((2,))],
+        compiler_params=pltpu.CompilerParams(vmem_limit_bytes=60 * 1024 * 1024),
+    )(*out)
+    return (u[None], v[None], mix, bias, gain_g[0], shift_g[0])
 
 
 def solution(mesh):

time: 61.5 us -> 58.7 us (0.954)
  local copies, waits for them, and re-layouts: 8.73 us -> 0 us
  Pallas kernels: 51.9 us -> 57.8 us
    unnamed x19 -> x0, local copies, waits for them, and re-layouts: 8.73 us -> none
    pallas_call x0 -> x1, Pallas kernels: none -> 3.65 us  [per_device(): pl.pallas_call(finish, out_shape=(jax.ShapeDtypeStruct((tok, half), bf16)...]
    pallas_call x1, Pallas kernels: 51.9 us -> 54.2 us  [per_device(): pl.pallas_call(functools.partial(kernel, (tok, width, groups, span, dp_co...]
where the time goes in v2:
time: 58.7 us; the launch traced here: 58.5 us
  Pallas kernels  57.8 us (98%)
  between operations  0.64 us (1%)
    pallas_call x1, Pallas kernels, per_device(): pl.pallas_call(functools.partial(kernel, (tok, width, groups, span, dp_co...  54.2 us
    pallas_call x1, Pallas kernels, per_device(): pl.pallas_call(finish, out_shape=(jax.ShapeDtypeStruct((tok, half), bf16)...  3.65 us

profile of v2, /device:TPU:0, one launch (start us, length us, event | category | flops | bytes accessed | tf_op | source)
XLA Modules:
  0.0 58.5 jit_solution(6795285589565451178)
XLA Ops:
  0.6 54.2 %shard_map.118 = (bf16[128,3072]{1,0:T(8,128)(2,1)}, bf16[128,3072]{1,0:T(8,128)(2,1)}, bf16[4,128,512]{2,1,0:T(8,128)(2,1)}, f32[16,512]{1,0:T(8,128)}) custom-call(bf16[128,3072]{1,0:T(8,128)(2,1)} %bitcast.9, bf16[128,3072]{1,0:T(8,128)(2,1)} %bitcast.10, bf16[128,3072]{1,0:T(8,128)(2,1)} %bitcast.11, f32[1,3072]{1,0:T(1,128)} %bitcast.12, ...), custom_call_target="tpu_custom_call" | custom-call | tf_op jit(solution)/shard_map/pallas_call | solution.py:390
  54.8 3.7 %shard_map.119 = (bf16[128,3072]{1,0:T(8,128)(2,1)}, bf16[128,3072]{1,0:T(8,128)(2,1)}, f32[128,4,512]{2,1,0:T(4,128)}, f32[4,512]{1,0:T(4,128)}, f32[1,3072]{1,0:T(1,128)}, /*index=5*/f32[1,3072]{1,0:T(1,128)}) custom-call(bf16[128,3072]{1,0:T(8,128)(2,1)} %get-tuple-element.16.u_in, bf16[128,3072]{1,0:T(8,128)(2,1)} %get-tuple-element.17.v_in, ...), custom_call_target="tpu_custom_call" | custom-call | tf_op jit(solution)/shard_map/pallas_call | solution.py:413

commit v3 on v2

--- a/solution.py
+++ b/solution.py
@@ -257,6 +257,17 @@
         preferred_element_type=f32,
     )[0:1]
 
+    def total(ref, count):
+        out = ref[0].astype(f32)
+        for i in range(1, count):
+            out = out + ref[i].astype(f32)
+        return out
+
+    go_t.arrive()
+    dp_sum[...] = total(term_r, dp_count).astype(bf16)
+    go_s.start()
+    span_r[my_span] = dp_sum[...]
+
     go_b.arrive()
 
     @pl.loop(0, tok // CHUNK)
@@ -286,17 +297,6 @@
         vec_s[0, 2 * parts + g : 2 * parts + g + 1, :] = jnp.where(k == g, bias_sum, 0.0)
     go_va.start()
     vec_a[d] = vec_s[0]
-
-    def total(ref, count):
-        out = ref[0].astype(f32)
-        for i in range(1, count):
-            out = out + ref[i].astype(f32)
-        return out
-
-    go_t.arrive()
-    dp_sum[...] = total(term_r, dp_count).astype(bf16)
-    go_s.start()
-    span_r[my_span] = dp_sum[...]
 
     go_va.arrive()
     vec_s[1] = total(vec_a, dp_count)

time: 58.7 us -> 58.5 us (level)
  no operation moved by 1% of the time
where the time goes in v3:
time: 58.5 us; the launch traced here: 58.3 us
  Pallas kernels  57.7 us (99%)
  between operations  0.64 us (1%)
    pallas_call x1, Pallas kernels, per_device(): pl.pallas_call(functools.partial(kernel, (tok, width, groups, span, dp_co...  54 us
    pallas_call x1, Pallas kernels, per_device(): pl.pallas_call(finish, out_shape=(jax.ShapeDtypeStruct((tok, half), bf16)...  3.65 us

profile of v3, /device:TPU:0, one launch (start us, length us, event | category | flops | bytes accessed | tf_op | source)
XLA Modules:
  0.0 58.3 jit_solution(2520590516789577024)
XLA Ops:
  0.6 54.0 %shard_map.118 = (bf16[128,3072]{1,0:T(8,128)(2,1)}, bf16[128,3072]{1,0:T(8,128)(2,1)}, bf16[4,128,512]{2,1,0:T(8,128)(2,1)}, f32[16,512]{1,0:T(8,128)}) custom-call(bf16[128,3072]{1,0:T(8,128)(2,1)} %bitcast.9, bf16[128,3072]{1,0:T(8,128)(2,1)} %bitcast.10, bf16[128,3072]{1,0:T(8,128)(2,1)} %bitcast.11, f32[1,3072]{1,0:T(1,128)} %bitcast.12, ...), custom_call_target="tpu_custom_call" | custom-call | tf_op jit(solution)/shard_map/pallas_call | solution.py:390
  54.7 3.7 %shard_map.119 = (bf16[128,3072]{1,0:T(8,128)(2,1)}, bf16[128,3072]{1,0:T(8,128)(2,1)}, f32[128,4,512]{2,1,0:T(4,128)}, f32[4,512]{1,0:T(4,128)}, f32[1,3072]{1,0:T(1,128)}, /*index=5*/f32[1,3072]{1,0:T(1,128)}) custom-call(bf16[128,3072]{1,0:T(8,128)(2,1)} %get-tuple-element.16.u_in, bf16[128,3072]{1,0:T(8,128)(2,1)} %get-tuple-element.17.v_in, ...), custom_call_target="tpu_custom_call" | custom-call | tf_op jit(solution)/shard_map/pallas_call | solution.py:413
